TPU v7x, 32 devices: a whole 2x2x4 slice. The times are simulated.
32 devices in a mesh: sp: 16 (over z, y, x), tp: 2 (over core).
Axes of the slice: x: 2, y: 2, z: 4, core: 2. Of those that a mesh axis runs over, the one named last changes fastest.
Arguments:
- residual: bfloat16 [3072, 2048], P(('sp', 'tp')), may hold values from -6 to 6
- queries: bfloat16 [3072, 1024], P('sp', 'tp'), may hold values from -6 to 6
- key_pairs: bfloat16 [3072, 1024], P('sp', 'tp'), may hold values from -6 to 6
- values: bfloat16 [3072, 1024], P('sp', 'tp'), may hold values from -6 to 6
- second_weight: float32 [8], P('tp'), may hold values from 0.3 to 0.8
- head_gain: float32 [1024], P('tp'), may hold values from 0.1 to 1.9
- out_weight: bfloat16 [1024, 2048], P('tp'), may hold values from -0.1875 to 0.1875
- norm_gain: float32 [2048], replicated, may hold values from 0.1 to 1.9
- up_weight: bfloat16 [2048, 5632], P('sp', 'tp'), may hold values from -0.125 to 0.125
- gate_weight: bfloat16 [2048, 5632], P('sp', 'tp'), may hold values from -0.125 to 0.125
- conv_weight: float32 [3, 5632], P(None, 'tp'), may hold values from -3.5 to 3.5
- conv_bias: float32 [5632], P('tp'), may hold values from -3 to 3
- down_weight: bfloat16 [5632, 2048], P('tp', 'sp'), may hold values from -0.078125 to 0.078125
Outputs:
- layer_out: bfloat16 [3072, 2048], P(('sp', 'tp'))
All inputs are finite; a program needn't handle non-finite values.
Results may differ from a plain program's by a relative error of at most 0.017.
Values may be sent and summed in bfloat16 or wider, within the bound.
A program may use at most 128 MiB of HBM per device.

v0:
```python
import jax
import jax.numpy as jnp
from jax import lax
from jax.sharding import PartitionSpec as P

HD = 64
VD = 128
eps = 1e-05
neg_fill = -1e30


def from_behind(value, axis, steps):
    count = lax.axis_size(axis)
    leading, last = (max(0, -steps), min(count, count - steps))
    return lax.ppermute(value, axis, [(source, source + steps) for source in range(leading, last)])


def normalize(rows_in, gain):
    values_f = rows_in.astype(jnp.float32)
    scale_inv = lax.rsqrt(jnp.mean(values_f * values_f, axis=-1, keepdims=True) + eps)
    return (values_f * scale_inv * gain).astype(jnp.bfloat16)


def local(
    residual,
    queries,
    key_pairs,
    values,
    second_weight,
    head_gain,
    out_weight,
    norm_gain,
    up_weight,
    gate_weight,
    conv_weight,
    conv_bias,
    down_weight,
):
    tok_rows = queries.shape[0]
    head_count = second_weight.shape[0]
    ff_local = up_weight.shape[1]
    sp_index = lax.axis_index("sp")
    query = queries.reshape(tok_rows, head_count, 2, HD)
    query_pos = sp_index * tok_rows + jnp.arange(tok_rows)
    last_query = (sp_index + 1) * tok_rows
    initial = (
        jnp.full((head_count, 2, tok_rows), neg_fill, jnp.float32),
        jnp.zeros((head_count, 2, tok_rows), jnp.float32),
        jnp.zeros((head_count, 2, tok_rows, VD), jnp.float32),
    )
    key_piece = lax.all_gather(key_pairs, "sp", axis=0, tiled=True)
    value_piece = lax.all_gather(values, "sp", axis=0, tiled=True)
    piece_len = key_piece.shape[0]

    def compute(state_in):
        maxima, totals, weighted = state_in
        key_rows = key_piece.reshape(piece_len, head_count, 2, HD)
        value_rows = value_piece.reshape(piece_len, head_count, VD)
        scores = jnp.einsum(
            "qhmd,khmd->hmqk", query, key_rows, preferred_element_type=jnp.float32
        ) * HD ** (-0.5)
        visible = jnp.arange(piece_len)[None, :] <= query_pos[:, None]
        scores = jnp.where(visible, scores, neg_fill)
        new_max = jnp.maximum(maxima, jnp.max(scores, axis=-1))
        exp_scores = jnp.where(visible, jnp.exp(scores - new_max[..., None]), jnp.float32(0.0))
        totals = jnp.sum(exp_scores, axis=-1)
        weighted = jnp.einsum(
            "hmqk,khe->hmqe",
            exp_scores.astype(jnp.bfloat16),
            value_rows,
            preferred_element_type=jnp.float32,
        )
        return (new_max, totals, weighted)

    def keep_state(state_in):
        return state_in

    maxima, totals, weighted = lax.cond(jnp.int32(0) < last_query, compute, keep_state, initial)
    diff = (
        weighted[:, 0] / totals[:, 0, :, None]
        - second_weight[:, None, None] * weighted[:, 1] / totals[:, 1, :, None]
    )
    diff = jnp.transpose(diff, (1, 0, 2))
    scale_inv = lax.rsqrt(jnp.mean(diff * diff, axis=-1, keepdims=True) + eps)
    attended = (
        (diff * scale_inv * head_gain.reshape(head_count, VD) * 0.8)
        .reshape(tok_rows, head_count * VD)
        .astype(jnp.bfloat16)
    )
    proj = lax.psum_scatter(
        jnp.dot(attended, out_weight, preferred_element_type=jnp.float32).astype(jnp.bfloat16),
        "tp",
        scatter_dimension=0,
        tiled=True,
    )
    mid = (residual.astype(jnp.float32) + proj.astype(jnp.float32)).astype(jnp.bfloat16)
    normed_all = lax.all_gather(normalize(mid, norm_gain), "tp", axis=0, tiled=True)
    up_sum = jnp.dot(
        normed_all,
        lax.all_gather(up_weight, "sp", axis=0, tiled=True),
        preferred_element_type=jnp.float32,
    )
    gate_sum = jnp.dot(
        normed_all,
        lax.all_gather(gate_weight, "sp", axis=0, tiled=True),
        preferred_element_type=jnp.float32,
    )
    up_proj = up_sum.astype(jnp.bfloat16)
    gate_proj = gate_sum.astype(jnp.bfloat16)
    taps = conv_weight.shape[0]
    rim_rows = from_behind(up_proj[tok_rows - (taps - 1) :], "sp", 1)
    extended = jnp.concatenate((rim_rows, up_proj), axis=0)
    conv_out = jnp.zeros((tok_rows, ff_local), jnp.float32) + conv_bias[None, :]
    for tap in range(taps):
        conv_out = conv_out + conv_weight[tap][None, :] * extended[tap : tap + tok_rows].astype(
            jnp.float32
        )
    hidden = (jax.nn.silu(conv_out) * gate_proj.astype(jnp.float32)).astype(jnp.bfloat16)
    down_all = lax.all_gather(down_weight, "sp", axis=1, tiled=True)
    ffn_out = lax.psum_scatter(
        jnp.dot(hidden, down_all, preferred_element_type=jnp.float32).astype(jnp.bfloat16),
        "tp",
        scatter_dimension=0,
        tiled=True,
    )
    return (mid.astype(jnp.float32) + ffn_out.astype(jnp.float32)).astype(jnp.bfloat16)


def solution(mesh):
    return jax.shard_map(
        local,
        mesh=mesh,
        in_specs=(
            P(("sp", "tp"), None),
            P("sp", "tp"),
            P("sp", "tp"),
            P("sp", "tp"),
            P("tp"),
            P("tp"),
            P("tp", None),
            P(),
            P("sp", "tp"),
            P("sp", "tp"),
            P(None, "tp"),
            P("tp"),
            P("tp", "sp"),
        ),
        out_specs=P(("sp", "tp"), None),
        check_vma=False,
    )
```

profile of v0, /device:TPU:0, one launch (start us, length us, event | category | flops | bytes accessed | tf_op | source)
XLA Modules:
  0.0 705.0 jit_solution(9887044699763358971)
XLA Ops:
  6.5 0.7 all-gather.6.cloned.1.call-update
  7.3 0.7 all-gather.8.cloned.1.call-update
  8.0 0.0 reduce-scatter.3.cloned.1.call-start
  8.1 72.7 %all-gather.6.cloned.1.call-done = bf16[3072,512]{1,0:T(8,128)(2,1)} async-done(((bf16[192,512]{1,0:T(8,128)(2,1)}), bf16[3072,512]{1,0:T(8,128)(2,1)}) %all-gather.6.cloned.1.call-update) | async-done | bytes 3145744 | tf_op jit(solution)/shard_map/all_gather | solution.py:51
  80.7 69.2 %all-gather.8.cloned.1.call-done = bf16[3072,512]{1,0:T(8,128)(2,1)} async-done(((bf16[192,512]{1,0:T(8,128)(2,1)}), bf16[3072,512]{1,0:T(8,128)(2,1)}) %all-gather.8.cloned.1.call-update) | async-done | bytes 3145744 | tf_op jit(solution)/shard_map/all_gather | solution.py:52
  150.0 45.3 %conditional.1 = (f32[4,2,192]{2,1,0:T(2,128)S(1)}, f32[4,2,192,128]{3,2,1,0:T(8,128)S(1)}) conditional(s32[]{:T(128)} %convert_element_type.62, () %tuple.13, (s32[]{:T(128)}, s32[192]{0:T(256)S(1)}, bf16[192,512]{1,0:T(8,128)(2,1)}, bf16[3072,512]{1,0:T(8,128)(2,1)}, bf16[3072,512]{1,0:T(8,128)(2,1)}) %tuple.14), branch_computations={%region_0.0_spmd, %region_1.4_spmd} | conditional | flops 1873869568 | bytes 80058688 | solution.py:78
  150.0 0.4 iota_compare_fusion
  150.4 4.8 copy.26
  155.2 0.1 copy.25
  155.3 11.8 %fusion = (f32[4,2,192]{2,1,0:T(2,128)S(1)}, f32[4,2,192,3072]{3,2,1,0:T(8,128)}) fusion(pred[192,3072]{1,0:T(8,128)(4,1)S(1)} %iota_compare_fusion, bf16[192,4,2,64]{0,3,2,1:T(8,128)(2,1)S(1)} %bitcast.44, bf16[3072,4,2,64]{0,3,2,1:T(8,128)(2,1)} %bitcast.42), kind=kOutput, calls=%fused_computation.2 | convolution fusion | flops 618134016 | bytes 22812672 | tf_op jit(solution)/shard_map/cond/branch_1_fun/qhmd,khmd->hmqk/dot_general | solution.py:59
  167.1 5.5 reshape.37
  172.6 10.7 %fusion.3 = f32[4,2,192,128]{3,2,1,0:T(8,128)S(1)} fusion(f32[4,2,192,3072]{3,2,1,0:T(8,128)} %get-tuple-element.52, f32[4,2,192]{2,1,0:T(2,128)S(1)} %broadcast_maximum_fusion, pred[192,3072]{1,0:T(8,128)(4,1)S(1)} %iota_compare_fusion, bf16[3072,4,128,1]{2,1,0,3:T(4,128)(2,1)} %bitcast.43), kind=kOutput, calls=%fused_computation.5 | convolution fusion | flops 1231552512 | bytes 23402496 | tf_op jit(solution)/shard_map/cond/branch_1_fun/hmqk,khe->hmqe/dot_general | solution.py:67
  183.3 11.9 %fusion.2 = f32[4,2,192]{2,1,0:T(2,128)S(1)} fusion(f32[4,2,192,3072]{3,2,1,0:T(8,128)} %get-tuple-element.52, f32[4,2,192]{2,1,0:T(2,128)S(1)} %broadcast_maximum_fusion, pred[192,3072]{1,0:T(8,128)(4,1)S(1)} %iota_compare_fusion), kind=kLoop, calls=%fused_computation.4 | loop fusion | flops 23591424 | bytes 19476480 | tf_op jit(solution)/shard_map/cond/branch_1_fun/reduce_sum | solution.py:66
  195.3 0.5 multiply_reduce_fusion
  195.8 1.5 convolution_convert_fusion.3
  197.4 0.0 all-gather.10.cloned.1.call-start
  197.4 0.5 all-gather.10.cloned.1.call-update
  198.0 0.5 all-gather.12.cloned.1.call-update
  198.6 0.5 all-gather.14.cloned.1.call-update
  199.1 5.1 reduce-scatter.3.cloned.1.call-done
  204.2 1.2 fusion.20
  205.5 1.2 fusion.22
  206.6 2.4 all_gather.20
  209.0 140.4 %all-gather.10.cloned.1.call-done = bf16[2048,2816]{1,0:T(8,128)(2,1)} async-done(((bf16[128,2816]{1,0:T(8,128)(2,1)}), bf16[2048,2816]{1,0:T(8,128)(2,1)}) %all-gather.10.cloned.1.call-update) | async-done | bytes 11534352 | tf_op jit(solution)/shard_map/all_gather | solution.py:100
  349.4 6.7 convolution_convert_fusion.1
  356.1 3.4 collective-permute-start
  359.5 0.1 slice_reduce_fusion.2
  359.6 132.0 %all-gather.12.cloned.1.call-done = bf16[2048,2816]{1,0:T(8,128)(2,1)} async-done(((bf16[128,2816]{1,0:T(8,128)(2,1)}), bf16[2048,2816]{1,0:T(8,128)(2,1)}) %all-gather.12.cloned.1.call-update) | async-done | bytes 11534352 | tf_op jit(solution)/shard_map/all_gather | solution.py:105
  491.6 182.8 %all-gather.14.cloned.1.call-done = bf16[2816,2048]{1,0:T(8,128)(2,1)} async-done(((bf16[2816,128]{1,0:T(8,128)(2,1)}), bf16[2816,2048]{1,0:T(8,128)(2,1)}) %all-gather.14.cloned.1.call-update) | async-done | bytes 11534352 | tf_op jit(solution)/shard_map/all_gather | solution.py:119
  674.5 15.2 %convolution_convert_fusion.2 = bf16[192,2048]{1,0:T(8,128)(2,1)} fusion(bf16[2816,2048]{1,0:T(8,128)(2,1)} %all-gather.14.cloned.1.call-done, bf16[192,2048]{1,0:T(8,128)(2,1)} %copy-done.4, bf16[2048,2816]{1,0:T(8,128)(2,1)} %all-gather.12.cloned.1.call-done, bf16[192,2816]{1,0:T(8,128)(2,1)} %copy-done.10, bf16[2,2816]{1,0:T(2,128)(2,1)S(1)} %collective-permute-done, ...), kind=kOutput, calls=%fused_computation.19 | convolution fusion | flops 4442013696 | bytes 25779200 | tf_op jit(solution)/shard_map/dot_general | solution.py:121
  689.7 6.5 reduce-scatter.5.cloned.1.call-done
  696.2 1.9 fusion.23
  (40 shorter events, 0.3 us)
Async XLA Ops:
  6.5 189.2 %copy-start = (bf16[512,2048]{1,0:T(8,128)(2,1)S(1)}, bf16[512,2048]{1,0:T(8,128)(2,1)}, u32[]{:S(2)}) copy-start(bf16[512,2048]{1,0:T(8,128)(2,1)} %param.21) | copy-start | bytes 6291460
  6.5 74.2 %all-gather.6.cloned.1.call-start = ((), (), s32[]{:S(2)}) async-start(), calls=%async_computation.2 | async-start | bytes 3342336 | tf_op jit(solution)/shard_map/all_gather | solution.py:51
  7.3 142.7 %all-gather.8.cloned.1.call-start = ((), (), s32[]{:S(2)}) async-start(), calls=%async_computation.3 | async-start | bytes 3342336 | tf_op jit(solution)/shard_map/all_gather | solution.py:52
  8.0 196.2 %reduce-scatter.3.cloned.1.call-start = ((), (), s32[]{:S(2)}) async-start(), calls=%async_computation.4 | async-start | bytes 1179648 | tf_op jit(solution)/shard_map/reduce_scatter | solution.py:90
  149.9 45.3 %copy-start.9 = (f32[4]{0:T(128)S(1)}, f32[4]{0:T(128)}, u32[]{:S(2)}) copy-start(f32[4]{0:T(128)} %param.19) | copy-start | bytes 52
  149.9 45.8 %copy-start.8 = (f32[512]{0:T(512)S(1)}, f32[512]{0:T(512)}, u32[]{:S(2)}) copy-start(f32[512]{0:T(512)} %param.20) | copy-start | bytes 6148
  150.3 4.8 copy-start.5
  195.7 8.5 %copy-start.2 = (bf16[96,2048]{1,0:T(8,128)(2,1)S(1)}, bf16[96,2048]{1,0:T(8,128)(2,1)}, u32[]{:S(2)}) copy-start(bf16[96,2048]{1,0:T(8,128)(2,1)} %param.15) | copy-start | bytes 1179652
  195.8 9.7 %copy-start.7 = (f32[2048]{0:T(1024)S(1)}, f32[2048]{0:T(1024)}, u32[]{:S(2)}) copy-start(f32[2048]{0:T(1024)} %param.22) | copy-start | bytes 24580
  197.4 152.0 %all-gather.10.cloned.1.call-start = ((), (), s32[]{:S(2)}) async-start(), calls=%async_computation.5 | async-start | bytes 12255232 | tf_op jit(solution)/shard_map/all_gather | solution.py:100
  197.9 293.7 %all-gather.12.cloned.1.call-start = ((), (), s32[]{:S(2)}) async-start(), calls=%async_computation.6 | async-start | bytes 12255232 | tf_op jit(solution)/shard_map/all_gather | solution.py:105
  198.5 475.9 %all-gather.14.cloned.1.call-start = ((), (), s32[]{:S(2)}) async-start(), calls=%async_computation.7 | async-start | bytes 12255232 | tf_op jit(solution)/shard_map/all_gather | solution.py:119
  199.1 497.1 %reduce-scatter.5.cloned.1.call-start = ((), (), s32[]{:S(2)}) async-start(), calls=%async_computation.8 | async-start | bytes 1179648 | tf_op jit(solution)/shard_map/reduce_scatter | solution.py:120
  209.0 147.1 %copy-start.4 = (bf16[192,2048]{1,0:T(8,128)(2,1)}, bf16[192,2048]{1,0:T(8,128)(2,1)S(1)}, u32[]{:S(2)}) copy-start(bf16[192,2048]{1,0:T(8,128)(2,1)S(1)} %all_gather.20) | copy-start | bytes 2359300
  209.0 150.5 %copy-start.6 = (f32[3,2816]{1,0:T(4,128)S(1)}, f32[3,2816]{1,0:T(4,128)}, u32[]{:S(2)}) copy-start(f32[3,2816]{1,0:T(4,128)} %param.25) | copy-start | bytes 101380
  209.0 465.5 %copy-start.11 = (f32[2816]{0:T(1024)S(1)}, f32[2816]{0:T(1024)}, u32[]{:S(2)}) copy-start(f32[2816]{0:T(1024)} %param.26) | copy-start | bytes 33796
  356.1 3.4 copy-start.10
  356.1 318.3 %collective-permute-start = (bf16[2,2816]{1,0:T(2,128)(2,1)S(1)}, bf16[2,2816]{1,0:T(2,128)(2,1)S(1)}, u32[]{:S(2)}, u32[]{:S(2)}) collective-permute-start(bf16[2,2816]{1,0:T(2,128)(2,1)S(1)} %slice.41), channel_id=1, source_target_pairs={{0,2},{2,4},{4,6},{6,8},{8,10},{10,12},{12,14},{14,16},{16,18},{18... | collective-permute-start | bytes 33800 | tf_op jit(solution)/shard_map/ppermute | solution.py:15
  674.5 21.8 %copy-start.3 = (bf16[96,2048]{1,0:T(8,128)(2,1)S(1)}, bf16[96,2048]{1,0:T(8,128)(2,1)}, u32[]{:S(2)}) copy-start(bf16[96,2048]{1,0:T(8,128)(2,1)} %reduce-scatter.3.cloned.1.call-done) | copy-start | bytes 1179652
  674.5 23.7 %copy-start.1 = (bf16[512,2048]{1,0:T(8,128)(2,1)S(1)}, bf16[512,2048]{1,0:T(8,128)(2,1)}, u32[]{:S(2)}) copy-start(bf16[512,2048]{1,0:T(8,128)(2,1)} %param.21) | copy-start | bytes 6291460
Sparse Core Ops, SparseCore 0:
  10.1 70.5 all-gather.5
  83.5 66.3 all-gather.7
  197.5 6.6 reduce-scatter.2
  206.8 142.5 all-gather.9
  352.0 139.5 all-gather.11
  494.2 180.2 all-gather.13
  689.8 6.3 reduce-scatter.4
where the time goes:
time: 706 us; the launch traced here: 705 us
  waiting for transfers between devices  612 us (87%)
  matrix products  45.9 us (7%)
  other arithmetic  17.1 us (2%)
  between operations  13.6 us (2%)
  local copies, waits for them, and re-layouts  10.6 us (2%)
    all_gather x1, waiting for transfers between devices, local(): down_all = lax.all_gather(down_weight, 'sp', axis=1, tiled=True)  183 us
    all_gather x1, waiting for transfers between devices, local(): lax.all_gather(up_weight, 'sp', axis=0, tiled=True)  140 us
    all_gather x1, waiting for transfers between devices, local(): lax.all_gather(gate_weight, 'sp', axis=0, tiled=True)  132 us
    all_gather x1, waiting for transfers between devices, local(): key_piece = lax.all_gather(key_pairs, 'sp', axis=0, tiled=True)  72.7 us
    all_gather x1, waiting for transfers between devices, local(): value_piece = lax.all_gather(values, 'sp', axis=0, tiled=True)  69.2 us
    dot_general x1, matrix products, local(): jnp.dot(hidden, down_all, preferred_element_type=jnp.float32)  15.2 us
  transfers between devices with their start and end apart: 8, of which 7 were waited for; matrix products, arithmetic and copies ran while one was open for 1% of the time, Pallas kernels for 0%

commit v1 on v0

--- a/solution.py
+++ b/solution.py
@@ -116,7 +116,7 @@
             jnp.float32
         )
     hidden = (jax.nn.silu(conv_out) * gate_proj.astype(jnp.float32)).astype(jnp.bfloat16)
-    down_all = lax.all_gather(down_weight, "sp", axis=1, tiled=True)
+    down_all = jnp.concatenate(lax.all_gather(down_weight, "sp"), axis=1)
     ffn_out = lax.psum_scatter(
         jnp.dot(hidden, down_all, preferred_element_type=jnp.float32).astype(jnp.bfloat16),
         "tp",

time: 706 us -> 666 us (0.943)
  waiting for transfers between devices: 612 us -> 556 us
  local copies, waits for them, and re-layouts: 10.6 us -> 25.8 us
    all_gather x1, waiting for transfers between devices: 183 us -> 132 us  [local(): down_all = jnp.concatenate(lax.all_gather(down_weight, 'sp'), axis=1)]
    reshape x0 -> x1, local copies, waits for them, and re-layouts: none -> 15.2 us  [local(): down_all = jnp.concatenate(lax.all_gather(down_weight, 'sp'), axis=1)]
  transfers between devices with their start and end apart: 8 -> 8, of which waited for: 7 -> 7; matrix products, arithmetic and copies ran while one was open for 1% -> 4% of each run, Pallas kernels for 0% -> 0%
where the time goes in v1:
time: 666 us; the launch traced here: 665 us
  waiting for transfers between devices  556 us (83%)
  matrix products  46.5 us (7%)
  local copies, waits for them, and re-layouts  25.8 us (4%)
  other arithmetic  17.1 us (3%)
  between operations  13.6 us (2%)
    all_gather x1, waiting for transfers between devices, local(): lax.all_gather(up_weight, 'sp', axis=0, tiled=True)  140 us
    all_gather x1, waiting for transfers between devices, local(): down_all = jnp.concatenate(lax.all_gather(down_weight, 'sp'), axis=1)  132 us
    all_gather x1, waiting for transfers between devices, local(): lax.all_gather(gate_weight, 'sp', axis=0, tiled=True)  127 us
    all_gather x1, waiting for transfers between devices, local(): key_piece = lax.all_gather(key_pairs, 'sp', axis=0, tiled=True)  72.7 us
    all_gather x1, waiting for transfers between devices, local(): value_piece = lax.all_gather(values, 'sp', axis=0, tiled=True)  69.2 us
    dot_general x1, matrix products, local(): jnp.dot(hidden, down_all, preferred_element_type=jnp.float32)  15.8 us
    reshape x1, local copies, waits for them, and re-layouts, local(): down_all = jnp.concatenate(lax.all_gather(down_weight, 'sp'), axis=1)  15.2 us
  transfers between devices with their start and end apart: 8, of which 7 were waited for; matrix products, arithmetic and copies ran while one was open for 4% of the time, Pallas kernels for 0%

profile of v1, /device:TPU:0, one launch (start us, length us, event | category | flops | bytes accessed | tf_op | source)
XLA Modules:
  0.0 665.0 jit_solution(90706076767632462)
XLA Ops:
  6.5 0.7 all-gather.7.cloned.1.call-update
  7.3 0.7 all-gather.9.cloned.1.call-update
  8.1 72.7 %all-gather.7.cloned.1.call-done = bf16[3072,512]{1,0:T(8,128)(2,1)} async-done(((bf16[192,512]{1,0:T(8,128)(2,1)}), bf16[3072,512]{1,0:T(8,128)(2,1)}) %all-gather.7.cloned.1.call-update) | async-done | bytes 3145744 | tf_op jit(solution)/shard_map/all_gather | solution.py:51
  80.7 69.2 %all-gather.9.cloned.1.call-done = bf16[3072,512]{1,0:T(8,128)(2,1)} async-done(((bf16[192,512]{1,0:T(8,128)(2,1)}), bf16[3072,512]{1,0:T(8,128)(2,1)}) %all-gather.9.cloned.1.call-update) | async-done | bytes 3145744 | tf_op jit(solution)/shard_map/all_gather | solution.py:52
  150.0 45.3 %conditional.1 = (f32[4,2,192]{2,1,0:T(2,128)S(1)}, f32[4,2,192,128]{3,2,1,0:T(8,128)S(1)}) conditional(s32[]{:T(128)} %convert_element_type.62, () %tuple.13, (s32[]{:T(128)}, s32[192]{0:T(256)S(1)}, bf16[192,512]{1,0:T(8,128)(2,1)}, bf16[3072,512]{1,0:T(8,128)(2,1)}, bf16[3072,512]{1,0:T(8,128)(2,1)}) %tuple.14), branch_computations={%region_0.0_spmd, %region_1.4_spmd} | conditional | flops 1873869568 | bytes 80058688 | solution.py:78
  150.0 0.4 iota_compare_fusion
  150.4 4.8 copy.32
  155.2 0.1 copy.31
  155.3 11.8 %fusion = (f32[4,2,192]{2,1,0:T(2,128)S(1)}, f32[4,2,192,3072]{3,2,1,0:T(8,128)}) fusion(pred[192,3072]{1,0:T(8,128)(4,1)S(1)} %iota_compare_fusion, bf16[192,4,2,64]{0,3,2,1:T(8,128)(2,1)S(1)} %bitcast.50, bf16[3072,4,2,64]{0,3,2,1:T(8,128)(2,1)} %bitcast.46), kind=kOutput, calls=%fused_computation.2 | convolution fusion | flops 618134016 | bytes 22812672 | tf_op jit(solution)/shard_map/cond/branch_1_fun/qhmd,khmd->hmqk/dot_general | solution.py:59
  167.1 5.5 reshape.41
  172.6 10.7 %fusion.3 = f32[4,2,192,128]{3,2,1,0:T(8,128)S(1)} fusion(f32[4,2,192,3072]{3,2,1,0:T(8,128)} %get-tuple-element.57, f32[4,2,192]{2,1,0:T(2,128)S(1)} %broadcast_maximum_fusion, pred[192,3072]{1,0:T(8,128)(4,1)S(1)} %iota_compare_fusion, bf16[3072,4,128,1]{2,1,0,3:T(4,128)(2,1)} %bitcast.49), kind=kOutput, calls=%fused_computation.5 | convolution fusion | flops 1231552512 | bytes 23402496 | tf_op jit(solution)/shard_map/cond/branch_1_fun/hmqk,khe->hmqe/dot_general | solution.py:67
  183.3 11.9 %fusion.2 = f32[4,2,192]{2,1,0:T(2,128)S(1)} fusion(f32[4,2,192,3072]{3,2,1,0:T(8,128)} %get-tuple-element.57, f32[4,2,192]{2,1,0:T(2,128)S(1)} %broadcast_maximum_fusion, pred[192,3072]{1,0:T(8,128)(4,1)S(1)} %iota_compare_fusion), kind=kLoop, calls=%fused_computation.4 | loop fusion | flops 23591424 | bytes 19476480 | tf_op jit(solution)/shard_map/cond/branch_1_fun/reduce_sum | solution.py:66
  195.3 0.5 multiply_reduce_fusion
  195.8 1.5 convolution_convert_fusion.3
  197.4 0.0 all-gather.11.cloned.1.call-start
  197.4 0.5 all-gather.11.cloned.1.call-update
  198.0 0.5 all-gather.15.cloned.1.call-update
  198.6 0.5 all-gather.13.cloned.1.call-update
  199.1 5.1 reduce-scatter.3.cloned.1.call-done
  204.2 1.2 fusion.20
  205.5 1.2 fusion.22
  206.6 2.4 all_gather.23
  209.0 140.4 %all-gather.11.cloned.1.call-done = bf16[2048,2816]{1,0:T(8,128)(2,1)} async-done(((bf16[128,2816]{1,0:T(8,128)(2,1)}), bf16[2048,2816]{1,0:T(8,128)(2,1)}) %all-gather.11.cloned.1.call-update) | async-done | bytes 11534352 | tf_op jit(solution)/shard_map/all_gather | solution.py:100
  349.4 6.7 %convolution_convert_fusion.1 = bf16[192,2816]{1,0:T(8,128)(2,1)S(1)} fusion(bf16[192,2048]{1,0:T(8,128)(2,1)S(1)} %all_gather.23, bf16[2048,2816]{1,0:T(8,128)(2,1)} %all-gather.11.cloned.1.call-done), kind=kOutput, calls=%fused_computation.17 | convolution fusion | flops 2215133184 | bytes 13402112 | tf_op jit(solution)/shard_map/dot_general | solution.py:98
  356.1 3.2 collective-permute-start
  359.3 0.1 slice_reduce_fusion.2
  359.4 132.2 %all-gather.15.cloned.1.call-done = bf16[45056,128]{1,0:T(8,128)(2,1)} async-done(((bf16[2816,128]{1,0:T(8,128)(2,1)}), bf16[45056,128]{1,0:T(8,128)(2,1)}) %all-gather.15.cloned.1.call-update) | async-done | bytes 11534352 | tf_op jit(solution)/shard_map/all_gather | solution.py:119
  491.6 15.2 %copy.35 = bf16[2816,16,128]{0,2,1:T(8,128)(2,1)} copy(bf16[2816,16,128]{2,0,1:T(8,128)(2,1)} %bitcast.47) | data formatting | bytes 23068672 | tf_op jit(solution)/shard_map/reshape | solution.py:119
  506.8 127.0 %all-gather.13.cloned.1.call-done = bf16[2048,2816]{1,0:T(8,128)(2,1)} async-done(((bf16[128,2816]{1,0:T(8,128)(2,1)}), bf16[2048,2816]{1,0:T(8,128)(2,1)}) %all-gather.13.cloned.1.call-update) | async-done | bytes 11534352 | tf_op jit(solution)/shard_map/all_gather | solution.py:105
  633.9 15.8 %convolution_convert_fusion.2 = bf16[192,2048]{1,0:T(8,128)(2,1)} fusion(bf16[2816,2048]{0,1:T(8,128)(2,1)} %bitcast.48, bf16[192,2048]{1,0:T(8,128)(2,1)} %copy-done.4, bf16[2048,2816]{1,0:T(8,128)(2,1)} %all-gather.13.cloned.1.call-done, bf16[192,2816]{1,0:T(8,128)(2,1)} %copy-done.10, bf16[2,2816]{1,0:T(2,128)(2,1)S(1)} %collective-permute-done, ...), kind=kOutput, calls=%fused_computation.19 | convolution fusion | flops 4442013696 | bytes 25779200 | tf_op jit(solution)/shard_map/dot_general | solution.py:121
  649.8 6.5 reduce-scatter.5.cloned.1.call-done
  656.3 1.9 fusion.23
  (41 shorter events, 0.3 us)
Async XLA Ops:
  6.5 189.2 %copy-start = (bf16[512,2048]{1,0:T(8,128)(2,1)S(1)}, bf16[512,2048]{1,0:T(8,128)(2,1)}, u32[]{:S(2)}) copy-start(bf16[512,2048]{1,0:T(8,128)(2,1)} %param.21) | copy-start | bytes 6291460
  6.5 74.2 %all-gather.7.cloned.1.call-start = ((), (), s32[]{:S(2)}) async-start(), calls=%async_computation.2 | async-start | bytes 3342336 | tf_op jit(solution)/shard_map/all_gather | solution.py:51
  7.3 142.7 %all-gather.9.cloned.1.call-start = ((), (), s32[]{:S(2)}) async-start(), calls=%async_computation.3 | async-start | bytes 3342336 | tf_op jit(solution)/shard_map/all_gather | solution.py:52
  8.0 196.2 %reduce-scatter.3.cloned.1.call-start = ((), (), s32[]{:S(2)}) async-start(), calls=%async_computation.4 | async-start | bytes 1179648 | tf_op jit(solution)/shard_map/reduce_scatter | solution.py:90
  149.9 45.3 %copy-start.9 = (f32[4]{0:T(128)S(1)}, f32[4]{0:T(128)}, u32[]{:S(2)}) copy-start(f32[4]{0:T(128)} %param.19) | copy-start | bytes 52
  149.9 45.8 %copy-start.8 = (f32[512]{0:T(512)S(1)}, f32[512]{0:T(512)}, u32[]{:S(2)}) copy-start(f32[512]{0:T(512)} %param.20) | copy-start | bytes 6148
  150.3 4.8 copy-start.5
  195.7 8.5 %copy-start.2 = (bf16[96,2048]{1,0:T(8,128)(2,1)S(1)}, bf16[96,2048]{1,0:T(8,128)(2,1)}, u32[]{:S(2)}) copy-start(bf16[96,2048]{1,0:T(8,128)(2,1)} %param.15) | copy-start | bytes 1179652
  195.8 9.7 %copy-start.7 = (f32[2048]{0:T(1024)S(1)}, f32[2048]{0:T(1024)}, u32[]{:S(2)}) copy-start(f32[2048]{0:T(1024)} %param.22) | copy-start | bytes 24580
  197.4 152.0 %all-gather.11.cloned.1.call-start = ((), (), s32[]{:S(2)}) async-start(), calls=%async_computation.5 | async-start | bytes 12255232 | tf_op jit(solution)/shard_map/all_gather | solution.py:100
  197.9 293.7 %all-gather.15.cloned.1.call-start = ((), (), s32[]{:S(2)}) async-start(), calls=%async_computation.8 | async-start | bytes 12255232 | tf_op jit(solution)/shard_map/all_gather | solution.py:119
  198.5 435.4 %all-gather.13.cloned.1.call-start = ((), (), s32[]{:S(2)}) async-start(), calls=%async_computation.6 | async-start | bytes 12255232 | tf_op jit(solution)/shard_map/all_gather | solution.py:105
  199.1 457.1 %reduce-scatter.5.cloned.1.call-start = ((), (), s32[]{:S(2)}) async-start(), calls=%async_computation.7 | async-start | bytes 1179648 | tf_op jit(solution)/shard_map/reduce_scatter | solution.py:120
  209.0 147.1 %copy-start.4 = (bf16[192,2048]{1,0:T(8,128)(2,1)}, bf16[192,2048]{1,0:T(8,128)(2,1)S(1)}, u32[]{:S(2)}) copy-start(bf16[192,2048]{1,0:T(8,128)(2,1)S(1)} %all_gather.23) | copy-start | bytes 2359300
  209.0 150.3 %copy-start.6 = (f32[3,2816]{1,0:T(4,128)S(1)}, f32[3,2816]{1,0:T(4,128)}, u32[]{:S(2)}) copy-start(f32[3,2816]{1,0:T(4,128)} %param.25) | copy-start | bytes 101380
  356.1 3.2 copy-start.10
  356.1 277.8 %collective-permute-start = (bf16[2,2816]{1,0:T(2,128)(2,1)S(1)}, bf16[2,2816]{1,0:T(2,128)(2,1)S(1)}, u32[]{:S(2)}, u32[]{:S(2)}) collective-permute-start(bf16[2,2816]{1,0:T(2,128)(2,1)S(1)} %slice.41), channel_id=1, source_target_pairs={{0,2},{2,4},{4,6},{6,8},{8,10},{10,12},{12,14},{14,16},{16,18},{18... | collective-permute-start | bytes 33800 | tf_op jit(solution)/shard_map/ppermute | solution.py:15
  491.6 142.3 %copy-start.11 = (f32[2816]{0:T(1024)S(1)}, f32[2816]{0:T(1024)}, u32[]{:S(2)}) copy-start(f32[2816]{0:T(1024)} %param.26) | copy-start | bytes 33796
  633.9 22.4 %copy-start.3 = (bf16[96,2048]{1,0:T(8,128)(2,1)S(1)}, bf16[96,2048]{1,0:T(8,128)(2,1)}, u32[]{:S(2)}) copy-start(bf16[96,2048]{1,0:T(8,128)(2,1)} %reduce-scatter.3.cloned.1.call-done) | copy-start | bytes 1179652
  633.9 24.3 %copy-start.1 = (bf16[512,2048]{1,0:T(8,128)(2,1)S(1)}, bf16[512,2048]{1,0:T(8,128)(2,1)}, u32[]{:S(2)}) copy-start(bf16[512,2048]{1,0:T(8,128)(2,1)} %param.21) | copy-start | bytes 6291460
Sparse Core Ops, SparseCore 0:
  10.1 70.5 all-gather.6
  83.5 66.3 all-gather.8
  197.5 6.6 reduce-scatter.2
  206.8 142.5 all-gather.10
  352.0 139.5 all-gather.14
  494.2 139.5 all-gather.12
  649.9 6.3 reduce-scatter.4
